TPU v7x, 1024 devices: a whole 4x4x32 slice. The times are simulated.
1024 devices in a mesh: sp: 32 (over z), tp: 4 (over y), dp: 8 (over x, core).
Axes of the slice: x: 4, y: 4, z: 32, core: 2. Of those that a mesh axis runs over, the one named last changes fastest.
Arguments:
- latent: bfloat16 [32768, 2048], P(('dp', 'sp', 'tp')), parts along dimension 0, may hold values from -6 to 6
- cond: bfloat16 [16384], P('dp'), parts along dimension 0, may hold values from -6 to 6
- context: bfloat16 [4096, 2048], P(('dp', 'sp')), parts along dimension 0, may hold values from -6 to 6
- context_cond: bfloat16 [2048], replicated, may hold values from -6 to 6
- modulation: bfloat16 [2048, 6144], P(('sp', 'tp')), may hold values from -0.125 to 0.125
- norm_gain: bfloat16 [2048], replicated, may hold values from 0.099609375 to 1.8984375
- w_x: bfloat16 [2048, 1024], P(None, 'tp'), may hold values from -0.125 to 0.125
- w_gate: bfloat16 [2048, 1024], P(None, 'tp'), may hold values from -0.125 to 0.125
- w_b: bfloat16 [2048, 256], P(None, 'tp'), may hold values from -0.125 to 0.125
- w_c: bfloat16 [2048, 256], P(None, 'tp'), may hold values from -0.125 to 0.125
- w_dt: bfloat16 [2, 2048, 16], P(None, None, 'tp'), may hold values from -0.125 to 0.125
- conv_x: bfloat16 [4, 1024], P(None, 'tp'), may hold values from -3 to 3
- conv_b: bfloat16 [4, 256], P(None, 'tp'), may hold values from -3 to 3
- conv_c: bfloat16 [4, 256], P(None, 'tp'), may hold values from -3 to 3
- decay_rate: float32 [2, 16], P(None, 'tp'), may hold values from 0 to 0.04
- decay_extra: float32 [32768, 16], P(('dp', 'sp'), 'tp'), parts along dimension 0, may hold values from -2 to 0
- out_gain: bfloat16 [1024], P('tp'), may hold values from 0.099609375 to 1.8984375
- w_out: bfloat16 [1024, 2048], replicated, may hold values from -0.1875 to 0.1875
Outputs:
- mixed: bfloat16 [32768, 2048], P(('dp', 'sp', 'tp')), parts along dimension 0
There are 8 independent parts, one for each index of `dp`. A program takes and returns all parts, laid end to end along the dimension named above; an argument that names none is the same for every part. Nothing has to cross between parts.
All inputs are finite; a program needn't handle non-finite values.
Results may differ from a plain program's by a relative error of at most 0.007.
Values may be sent and summed in bfloat16 or wider, within the bound.
No kernel may reach another device: no remote copies, remote signals or barrier semaphores. Data moves between devices by JAX's collectives and lax.ppermute only.
A program may use at most 64 MiB of HBM per device.

v0:
```python
import jax
import jax.numpy as jnp
import numpy as np
from jax import lax
from jax.experimental import pallas as pl
from jax.experimental.pallas import tpu as pltpu
from jax.sharding import Mesh
from jax.sharding import PartitionSpec as P


HEAD_DIM = 64
STATE = 64
ROW_EPS = 1e-06
GROUP_EPS = 1e-05
HIGHEST = lax.Precision.HIGHEST
F32 = jnp.float32
BF16 = jnp.bfloat16
PAD = 8

SP = ("za", "zb", "zc")
NEAR = ("zb", "zc")
MOD_NEAR = ("zc", "tp")
MOD_FAR = ("za", "zb")


def exchange(x, axis):
    return lax.all_to_all(x, axis, 0, 0, tiled=True)


def share(x, axis):
    n = lax.axis_size(axis)
    full = jnp.broadcast_to(x[None], (n, *x.shape)).reshape(n * x.shape[0], *x.shape[1:])
    return exchange(full, axis).reshape(n, *x.shape)


def ring_rows(x):
    n = lax.axis_size("tp")
    moved = [x] + [lax.ppermute(x, "tp", [(i, (i + k) % n) for i in range(n)]) for k in range(1, n)]
    moved = jnp.stack(moved)
    place = lax.axis_index("tp")
    return jnp.stack([lax.dynamic_index_in_dim(moved, (place - t) % n, 0, False) for t in range(n)])


def split_hi_lo(x):
    hi = lax.reduce_precision(x, 8, 7)
    return hi, x - hi


def whole(shape):
    return pl.BlockSpec(shape, lambda i: (0,) * len(shape))


def silu(v):
    return v / (1.0 + jnp.exp(-v))


def partial_kernel(first, cond, context_cond, modulation, out):
    share_rows, cols = modulation.shape
    width = cols // 3
    at = first[0] + lax.broadcasted_iota(jnp.int32, (share_rows, width), 0)
    pick = jnp.where(lax.broadcasted_iota(jnp.int32, (share_rows, width), 1) == at, 1.0, 0.0).astype(BF16)
    table = modulation[...]
    cut = width // (out.shape[0] // 5)
    for source, kinds in ((0, (0, 1, 2)), (1, (0, 1))):
        v = (cond, context_cond)[source][...].astype(F32).reshape(1, width)
        row = silu(v).astype(BF16)
        own = lax.dot_general(row, pick, (((1,), (1,)), ((), ())), preferred_element_type=F32).astype(BF16)
        sums = jnp.dot(own, table, preferred_element_type=F32)
        for kind in kinds:
            for n in range(width // cut):
                for r in range(2):
                    at = kind * width + n * cut + r * 128
                    out[n * 5 + 3 * source + kind, r : r + 1, :] = sums[0:1, at : at + 128]


def partial_mods(first, cond, context_cond, modulation, n):
    return pl.pallas_call(
        partial_kernel,
        grid=(1,),
        out_shape=jax.ShapeDtypeStruct((n * 5, 2, 128), F32),
        in_specs=[pl.BlockSpec(memory_space=pltpu.SMEM)] + [whole(v.shape) for v in (cond, context_cond, modulation)],
        out_specs=whole((n * 5, 2, 128)),
        name="partial_mods",
    )(first.astype(jnp.int32).reshape(1), cond, context_cond, modulation)


def mod_vectors(cond, context_cond, modulation, own_rows, held):
    share_rows = modulation.shape[0]
    width = modulation.shape[1] // 3
    n = lax.axis_size(MOD_NEAR)
    cut = width // n
    pairs = 5 * cut // 256
    first = lax.axis_index((*SP, "tp")) * share_rows
    part = partial_mods(first, cond, context_cond, modulation, n)
    part = jnp.sum(exchange(part, MOD_NEAR).reshape(n, pairs, 2, 128), axis=0)
    part, held = lax.optimization_barrier((part, held))
    far = share(part, MOD_FAR)
    gathered = ring_rows(own_rows)
    full = share(jnp.sum(far, axis=0), MOD_NEAR)
    return full.reshape(n, 5, cut).transpose(1, 0, 2).reshape(5, width), gathered, held


def modulated_norm(rows, norm_gain, shift_row, scale_row):
    values = rows.astype(F32)
    normed = values * lax.rsqrt(jnp.mean(values * values, axis=-1, keepdims=True) + ROW_EPS)
    return (normed * norm_gain.astype(F32) * (1.0 + scale_row) + shift_row).astype(BF16)


def conv(values, taps, first, length):
    total = jnp.zeros((length, values.shape[1]), F32)
    for k in range(4):
        total = total + taps[k].astype(F32) * values[first + k : first + k + length]
    return jax.nn.silu(total).astype(BF16)


def decay_block(ctx_total, lat_total):
    row = lax.broadcasted_iota(jnp.int32, (8, 1), 0)
    block = jnp.zeros((8, 128), F32)
    for k, total in enumerate((ctx_total, lat_total)):
        hi, lo = split_hi_lo(total)
        block = jnp.where(row == 2 * k, hi, jnp.where(row == 2 * k + 1, lo, block))
    return block.astype(BF16)


def wide(v):
    heads = v.shape[1] // 2
    v = v.reshape(v.shape[0], 2, heads).transpose(0, 2, 1)
    return jnp.repeat(v, HEAD_DIM, axis=2).reshape(v.shape[0], heads * 2 * HEAD_DIM)


def twice(x):
    heads = x.shape[1] // HEAD_DIM
    v = x.reshape(x.shape[0], heads, 1, HEAD_DIM)
    return jnp.broadcast_to(v, (x.shape[0], heads, 2, HEAD_DIM)).reshape(x.shape[0], heads * 2 * HEAD_DIM)


def running_sums(log_decay):
    length = log_decay.shape[0]
    heads = log_decay.shape[1] // 2
    i = jnp.arange(length)
    low = (i[:, None] >= i[None, :]).astype(F32)
    forward = jnp.dot(low, log_decay[:, :heads], precision=HIGHEST)
    backward = jnp.dot(low.T, log_decay[:, heads:], precision=HIGHEST)
    return jnp.concatenate([forward, backward], axis=1)


def end_states(xs, bmat, dt, running, total):
    weights = wide(jnp.exp(total - running) * dt)
    weighted = (twice(xs).astype(F32) * weights).astype(BF16)
    return lax.dot_general(bmat, weighted, (((0,), (0,)), ((), ())), preferred_element_type=F32)


def entry_sums(states, totals, f_lane):
    n = states.shape[0]
    m = lax.broadcasted_iota(jnp.int32, (n + 1, n, n, 1), 0)
    k = lax.broadcasted_iota(jnp.int32, (n + 1, n, n, 1), 1)
    j = lax.broadcasted_iota(jnp.int32, (n + 1, n, n, 1), 2)
    mb = jnp.where(m == n, -1, m)
    between = jnp.where(f_lane, (j > k) & (j < m), (j < k) & (j > mb))
    gap = jnp.sum(jnp.where(between, totals[None, None], 0.0), axis=2)
    ahead = jnp.where(f_lane, k[:, :, 0] < m[:, :, 0], k[:, :, 0] > mb[:, :, 0])
    factor = jnp.where(ahead, jnp.exp(gap), 0.0)
    sums = jnp.sum(factor[:, :, None] * states[None], axis=1)
    to_m = jnp.sum(jnp.where(ahead, totals[None], 0.0), axis=1)
    return sums, to_m


def entry_states(ctx_state, ctx_total, lat_state, lat_total):
    heads = ctx_total.shape[1] // 2
    n = lax.axis_size(NEAR)
    half = heads * STATE // n

    def pieces(state):
        v = state.reshape(STATE // half, half, heads, 128).transpose(2, 0, 1, 3)
        return v.reshape(n, half, 128)

    block = decay_block(
        *(jnp.repeat(wide(t).reshape(heads, 1, 128), STATE // half, axis=0) for t in (ctx_total, lat_total))
    )
    near = jnp.concatenate([pieces(ctx_state).astype(BF16), pieces(lat_state).astype(BF16), block], axis=1)
    near = exchange(near, NEAR).astype(F32)
    f_lane = lax.broadcasted_iota(jnp.int32, (1, 128), 1) < HEAD_DIM
    ctx_t = near[:, 2 * half] + near[:, 2 * half + 1]
    lat_t = near[:, 2 * half + 2] + near[:, 2 * half + 3]
    ctx_sums, ctx_to = entry_sums(near[:, :half], ctx_t, f_lane)
    lat_sums, lat_to = entry_sums(near[:, half : 2 * half], lat_t, f_lane)
    far = jnp.concatenate(
        [ctx_sums[n].astype(BF16), lat_sums[n].astype(BF16), decay_block(ctx_to[n:], lat_to[n:])], axis=0
    )
    far = share(far, "za").astype(F32)
    count = far.shape[0]
    start, _ = entry_sums(far[:, :half], far[:, 2 * half] + far[:, 2 * half + 1], f_lane)
    group, group_to = entry_sums(far[:, half : 2 * half], far[:, 2 * half + 2] + far[:, 2 * half + 3], f_lane)
    mine = (jnp.arange(count + 1) == lax.axis_index("za")).astype(F32)
    group = jnp.sum(mine[:, None, None] * group, axis=0)
    group_to = jnp.sum(mine[:, None] * group_to, axis=0)
    entry = jnp.exp(group_to) * start[count] + group
    back = (jnp.exp(lat_to[:n, None]) * entry + lat_sums[:n]).astype(BF16)
    back = exchange(back, NEAR)
    return back.reshape(heads, STATE, 128)


def program(
    latent,
    cond,
    context,
    context_cond,
    modulation,
    norm_gain,
    w_x,
    w_gate,
    w_b,
    w_c,
    w_dt,
    conv_x,
    conv_b,
    conv_c,
    decay_rate,
    decay_extra,
    out_gain,
    w_out,
):
    heads = w_dt.shape[2]
    head_cols = w_x.shape[1]
    tokens = decay_extra.shape[0]
    ctx_tokens = context.shape[0]
    count = lax.axis_size(SP)
    place = lax.axis_index(SP)
    up = [(i, i + 1) for i in range(count - 1)]
    down = [(i + 1, i) for i in range(count - 1)]
    low = lax.ppermute(jnp.concatenate([latent[-PAD:], context[-PAD:]]), SP, up)
    high = lax.ppermute(jnp.concatenate([latent[:PAD], context[:PAD]]), SP, down)
    upper = lax.broadcasted_iota(jnp.int32, (PAD, 1), 0) < PAD // 2
    own = jnp.concatenate([latent, jnp.where(upper, high[:PAD], low[:PAD])])
    context_rows = jnp.concatenate([low[PAD:], context, high[PAD:]])
    held = (conv_x, conv_b, conv_c, decay_rate, decay_extra, norm_gain, w_dt, out_gain)
    mods, gathered, held = mod_vectors(cond, context_cond, modulation, own, held)
    conv_x, conv_b, conv_c, decay_rate, decay_extra, norm_gain, w_dt, out_gain = held
    tokens_own = latent.shape[0]
    latent_rows = jnp.concatenate(
        [
            gathered[-1, tokens_own:],
            gathered[:, :tokens_own].reshape(tokens, latent.shape[1]),
            gathered[0, tokens_own:],
        ]
    )

    lat_len = tokens + 2 * PAD
    hidden = jnp.concatenate(
        [
            modulated_norm(latent_rows, norm_gain, mods[0], mods[1]),
            modulated_norm(context_rows, norm_gain, mods[3], mods[4]),
        ]
    )
    row = jnp.arange(hidden.shape[0])
    first = (row < PAD) | ((row >= lat_len) & (row < lat_len + PAD))
    last = ((row >= lat_len - PAD) & (row < lat_len)) | (row >= hidden.shape[0] - PAD)
    outside = (first & (place == 0)) | (last & (place == count - 1))
    inner = hidden[PAD : PAD + tokens]

    def project(rows, weight):
        return jnp.dot(rows, weight, preferred_element_type=F32).astype(BF16)

    p_x = jnp.where(outside[:, None], 0.0, project(hidden, w_x).astype(F32))
    p_b = jnp.where(outside[:, None], 0.0, project(hidden, w_b).astype(F32))
    p_c = jnp.where(outside[:lat_len, None], 0.0, project(hidden[:lat_len], w_c).astype(F32))
    p_dt = jax.nn.softplus(project(hidden, jnp.concatenate([w_dt[0], w_dt[1]], axis=1)).astype(F32))
    z = project(inner, w_gate).astype(F32)

    off = PAD - 2
    xs = conv(p_x, conv_x, off, tokens)
    bmat = conv(p_b, conv_b, off, tokens)
    cmat = conv(p_c, conv_c, off, tokens)
    ctx_xs = conv(p_x, conv_x, lat_len + off, ctx_tokens)
    ctx_b = conv(p_b, conv_b, lat_len + off, ctx_tokens)
    dt = p_dt[PAD : PAD + tokens]
    ctx_dt = p_dt[lat_len + PAD : lat_len + PAD + ctx_tokens]
    rate = decay_rate.reshape(1, 2 * heads)
    log_decay = -rate * dt + jnp.concatenate([decay_extra, decay_extra], axis=1)
    ctx_log_decay = -rate * ctx_dt
    running = running_sums(log_decay)
    ctx_running = running_sums(ctx_log_decay)
    total = jnp.sum(log_decay, axis=0, keepdims=True)
    ctx_total = jnp.sum(ctx_log_decay, axis=0, keepdims=True)
    entry = entry_states(
        end_states(ctx_xs, ctx_b, ctx_dt, ctx_running, ctx_total),
        ctx_total,
        end_states(xs, bmat, dt, running, total),
        total,
    )

    affinity = lax.dot_general(cmat, bmat, (((1,), (1,)), ((), ())), preferred_element_type=F32)
    i = jnp.arange(tokens)
    lower = i[:, None] >= i[None, :]
    upper = i[:, None] <= i[None, :]
    parts = []
    for h in range(heads):
        weights = jnp.zeros((tokens, tokens), F32)
        for d, mask in ((0, lower), (1, upper)):
            col = d * heads + h
            gap = running[:, col][:, None] - running[:, col][None, :]
            mixing = jnp.where(mask, jnp.exp(jnp.where(mask, gap, 0.0)), 0.0)
            weights = weights + mixing * dt[:, col][None, :]
        weights = (affinity * weights).astype(BF16)
        parts.append(jnp.dot(weights, xs[:, h * HEAD_DIM : (h + 1) * HEAD_DIM], preferred_element_type=F32))
    y = jnp.concatenate(parts, axis=1)
    for d in range(2):
        flat = entry[:, :, d * HEAD_DIM : (d + 1) * HEAD_DIM].transpose(1, 0, 2).reshape(STATE, heads * HEAD_DIM)
        decayed = jnp.repeat(jnp.exp(running[:, d * heads : (d + 1) * heads]), HEAD_DIM, axis=1)
        y = y + jnp.dot(cmat, flat, preferred_element_type=F32) * decayed
    gated = y * jax.nn.silu(z)
    mean_square = jnp.mean(gated * gated, axis=1, keepdims=True)
    normed = (gated * lax.rsqrt(mean_square + GROUP_EPS) * out_gain.astype(F32)).astype(BF16)
    tp_count = lax.axis_size("tp")
    stacked = normed.reshape(tp_count, tokens // tp_count, head_cols)
    full = lax.all_to_all(stacked, "tp", split_axis=0, concat_axis=2, tiled=True)[0]
    branch = jnp.dot(full, w_out, preferred_element_type=F32)
    return (latent.astype(F32) + mods[2] * branch).astype(BF16)


def solution(mesh):
    sp, tp, dp = (mesh.shape[a] for a in ("sp", "tp", "dp"))
    inner = Mesh(np.asarray(mesh.devices).reshape(sp // 8, 4, 2, tp, dp), (*SP, "tp", "dp"))
    in_specs = (
        P(("dp", *SP, "tp"), None),
        P("dp"),
        P(("dp", *SP), None),
        P(),
        P((*SP, "tp"), None),
        P(),
        P(None, "tp"),
        P(None, "tp"),
        P(None, "tp"),
        P(None, "tp"),
        P(None, None, "tp"),
        P(None, "tp"),
        P(None, "tp"),
        P(None, "tp"),
        P(None, "tp"),
        P(("dp", *SP), "tp"),
        P("tp"),
        P(),
    )
    out_specs = P(("dp", *SP, "tp"), None)
    return jax.shard_map(program, mesh=inner, in_specs=in_specs, out_specs=out_specs, check_vma=False)
```

profile of v0, /device:TPU:2, one launch (start us, length us, event | category | flops | bytes accessed | tf_op | source)
XLA Modules:
  0.0 181.5 jit_solution(16802934393498702694)
XLA Ops:
  0.0 2.3 %partial_mods.1 = f32[40,2,128]{2,1,0:T(2,128)} custom-call(s32[1]{0:T(128)} %bitcast.first, bf16[2048]{0:T(1024)(128)(2,1)} %cond.1, bf16[2048]{0:T(1024)(128)(2,1)} %context_cond.1, bf16[16,6144]{1,0:T(8,128)(2,1)} %modulation.1), custom_call_target="tpu_custom_call" | custom-call | tf_op jit(solution)/shard_map/partial_mods/pallas_call | solution.py:77
  2.3 5.8 %all-to-all-start = ((f32[40,2,128]{2,1,0:T(2,128)}), f32[40,2,128]{2,1,0:T(2,128)S(1)}, u32[]{:S(2)}, u32[]{:S(2)}) async-start(f32[40,2,128]{2,1,0:T(2,128)} %partial_mods.1), calls=%async_computation | async-start | bytes 81920 | tf_op jit(solution)/shard_map/all_to_all | solution.py:27
  8.1 0.8 fusion.136
  9.0 3.9 %collective-permute-start.1 = (bf16[16,2048]{1,0:T(8,128)(2,1)S(1)}, bf16[16,2048]{1,0:T(8,128)(2,1)S(1)}, u32[]{:S(2)}, u32[]{:S(2)}) collective-permute-start(bf16[16,2048]{1,0:T(8,128)(2,1)S(1)} %pad_maximum_fusion.13), channel_id=1, source_target_pairs={{0,32},{32,64},{64,96},{96,128},{128,160},{160,192},{192,224},{224... | collective-permute-start | bytes 196616 | tf_op jit(solution)/shard_map/ppermute | solution.py:231
  12.9 1.3 collective-permute-start
  15.0 4.0 %collective-permute-done = bf16[16,2048]{1,0:T(8,128)(2,1)S(1)} collective-permute-done((bf16[16,2048]{1,0:T(8,128)(2,1)S(1)}, bf16[16,2048]{1,0:T(8,128)(2,1)S(1)}, u32[]{:S(2)}, u32[]{:S(2)}) %collective-permute-start) | collective-permute-done | bytes 65568 | tf_op jit(solution)/shard_map/ppermute | solution.py:232
  19.2 4.9 %collective-permute-start.4 = (bf16[40,2048]{1,0:T(8,128)(2,1)S(1)}, bf16[40,2048]{1,0:T(8,128)(2,1)S(1)}, u32[]{:S(2)}, u32[]{:S(2)}) collective-permute-start(bf16[40,2048]{1,0:T(8,128)(2,1)S(1)} %get-tuple-element.42), channel_id=1, source_target_pairs={{0,24},{8,0},{16,8},{24,16},{1,25},{9,1},{17,9},{25,17},{2,26},{10... | collective-permute-start | bytes 491528 | tf_op jit(solution)/shard_map/ppermute | solution.py:38
  24.1 2.8 %collective-permute-start.3 = (bf16[40,2048]{1,0:T(8,128)(2,1)S(1)}, bf16[40,2048]{1,0:T(8,128)(2,1)S(1)}, u32[]{:S(2)}, u32[]{:S(2)}) collective-permute-start(bf16[40,2048]{1,0:T(8,128)(2,1)S(1)} %get-tuple-element.42), channel_id=1, source_target_pairs={{0,16},{8,24},{16,0},{24,8},{1,17},{9,25},{17,1},{25,9},{2,18},{10... | collective-permute-start | bytes 491528 | tf_op jit(solution)/shard_map/ppermute | solution.py:38
  26.9 2.8 %collective-permute-start.2 = (bf16[40,2048]{1,0:T(8,128)(2,1)S(1)}, bf16[40,2048]{1,0:T(8,128)(2,1)S(1)}, u32[]{:S(2)}, u32[]{:S(2)}) collective-permute-start(bf16[40,2048]{1,0:T(8,128)(2,1)S(1)} %get-tuple-element.42), channel_id=1, source_target_pairs={{0,8},{8,16},{16,24},{24,0},{1,9},{9,17},{17,25},{25,1},{2,10},{10... | collective-permute-start | bytes 491528 | tf_op jit(solution)/shard_map/ppermute | solution.py:38
  29.8 0.6 collective-permute-done.4
  30.5 3.0 %collective-permute-done.3 = bf16[40,2048]{1,0:T(8,128)(2,1)S(1)} collective-permute-done((bf16[40,2048]{1,0:T(8,128)(2,1)S(1)}, bf16[40,2048]{1,0:T(8,128)(2,1)S(1)}, u32[]{:S(2)}, u32[]{:S(2)}) %collective-permute-start.3) | collective-permute-done | bytes 163872 | tf_op jit(solution)/shard_map/ppermute | solution.py:38
  33.5 1.9 %collective-permute-done.2 = bf16[40,2048]{1,0:T(8,128)(2,1)S(1)} collective-permute-done((bf16[40,2048]{1,0:T(8,128)(2,1)S(1)}, bf16[40,2048]{1,0:T(8,128)(2,1)S(1)}, u32[]{:S(2)}, u32[]{:S(2)}) %collective-permute-start.2) | collective-permute-done | bytes 163872 | tf_op jit(solution)/shard_map/ppermute | solution.py:38
  35.7 0.2 fusion.2
  36.0 0.7 broadcast_in_dim.554
  36.6 27.1 %all-to-all-start.1 = ((f32[80,2,128]{2,1,0:T(2,128)}), f32[80,2,128]{2,1,0:T(2,128)S(1)}, u32[]{:S(2)}, u32[]{:S(2)}) async-start(f32[80,2,128]{2,1,0:T(2,128)} %bitcast.2), calls=%async_computation.1 | async-start | bytes 163840 | tf_op jit(solution)/shard_map/all_to_all | solution.py:27
  63.8 23.4 %all-to-all-done.1 = f32[80,2,128]{2,1,0:T(2,128)S(1)} async-done(((f32[80,2,128]{2,1,0:T(2,128)}), f32[80,2,128]{2,1,0:T(2,128)S(1)}, u32[]{:S(2)}, u32[]{:S(2)}) %all-to-all-start.1) | async-done | bytes 81952 | tf_op jit(solution)/shard_map/all_to_all | solution.py:27
  87.2 0.6 broadcast_in_dim.555
  87.8 3.3 %all-to-all-start.2 = ((f32[40,2,128]{2,1,0:T(2,128)}), f32[40,2,128]{2,1,0:T(2,128)S(1)}, u32[]{:S(2)}, u32[]{:S(2)}) async-start(f32[40,2,128]{2,1,0:T(2,128)} %bitcast.4), calls=%async_computation.2 | async-start | bytes 81920 | tf_op jit(solution)/shard_map/all_to_all | solution.py:27
  91.3 6.0 %all-to-all-done.2 = f32[40,2,128]{2,1,0:T(2,128)S(1)} async-done(((f32[40,2,128]{2,1,0:T(2,128)}), f32[40,2,128]{2,1,0:T(2,128)S(1)}, u32[]{:S(2)}, u32[]{:S(2)}) %all-to-all-start.2) | async-done | bytes 40992 | tf_op jit(solution)/shard_map/all_to_all | solution.py:27
  97.5 0.3 fusion.6
  97.9 0.3 compare_select_fusion
  98.7 0.2 fusion.143
  98.9 0.4 fusion.14
  99.7 0.4 fusion.8
  100.2 0.7 slice_bitcast_fusion.11
  101.7 0.5 slice_bitcast_fusion.18
  103.3 0.2 fusion.16
  103.6 0.7 pad_maximum_fusion.10
  104.2 3.4 %all-to-all-start.3 = ((bf16[8,72,128]{2,1,0:T(8,128)(2,1)}), bf16[8,72,128]{2,1,0:T(8,128)(2,1)S(1)}, u32[]{:S(2)}, u32[]{:S(2)}) async-start(bf16[8,72,128]{2,1,0:T(8,128)(2,1)} %pad_maximum_fusion.10), calls=%async_computation.3 | async-start | bytes 294912 | tf_op jit(solution)/shard_map/all_to_all | solution.py:27
  107.8 0.3 fusion.18
  108.1 0.6 slice_bitcast_fusion.19
  108.9 0.9 fusion.46
  109.8 0.9 fusion.48
  110.6 8.7 %all-to-all-done.3 = bf16[8,72,128]{2,1,0:T(8,128)(2,1)S(1)} async-done(((bf16[8,72,128]{2,1,0:T(8,128)(2,1)}), bf16[8,72,128]{2,1,0:T(8,128)(2,1)S(1)}, u32[]{:S(2)}, u32[]{:S(2)}) %all-to-all-start.3) | async-done | bytes 147488 | tf_op jit(solution)/shard_map/all_to_all | solution.py:27
  119.3 0.3 fusion.21
  120.1 0.6 broadcast_in_dim.615
  120.7 8.6 %all-to-all-start.4 = ((bf16[4,72,128]{2,1,0:T(8,128)(2,1)}), bf16[4,72,128]{2,1,0:T(8,128)(2,1)S(1)}, u32[]{:S(2)}, u32[]{:S(2)}) async-start(bf16[4,72,128]{2,1,0:T(8,128)(2,1)} %broadcast_in_dim.615), calls=%async_computation.4 | async-start | bytes 147456 | tf_op jit(solution)/shard_map/all_to_all | solution.py:27
  129.4 1.1 fusion.50
  130.4 21.9 %all-to-all-done.4 = bf16[4,72,128]{2,1,0:T(8,128)(2,1)S(1)} async-done(((bf16[4,72,128]{2,1,0:T(8,128)(2,1)}), bf16[4,72,128]{2,1,0:T(8,128)(2,1)S(1)}, u32[]{:S(2)}, u32[]{:S(2)}) %all-to-all-start.4) | async-done | bytes 73760 | tf_op jit(solution)/shard_map/all_to_all | solution.py:27
  152.9 0.6 fusion.28
  153.6 3.5 %all-to-all-start.5 = ((bf16[8,32,128]{2,1,0:T(8,128)(2,1)}), bf16[8,32,128]{2,1,0:T(8,128)(2,1)S(1)}, u32[]{:S(2)}, u32[]{:S(2)}) async-start(bf16[8,32,128]{2,1,0:T(8,128)(2,1)} %fusion.28), calls=%async_computation.5 | async-start | bytes 131072 | tf_op jit(solution)/shard_map/all_to_all | solution.py:27
  157.1 1.7 fusion.52
  158.8 0.3 fusion.12
  159.1 8.9 %all-to-all-done.5 = bf16[8,32,128]{2,1,0:T(8,128)(2,1)S(1)} async-done(((bf16[8,32,128]{2,1,0:T(8,128)(2,1)}), bf16[8,32,128]{2,1,0:T(8,128)(2,1)S(1)}, u32[]{:S(2)}, u32[]{:S(2)}) %all-to-all-start.5) | async-done | bytes 65568 | tf_op jit(solution)/shard_map/all_to_all | solution.py:27
  168.4 1.0 fusion.11
  169.4 0.2 multiply_reduce_fusion.4
  169.8 8.0 %all_to_all.46 = bf16[4,32,256]{2,1,0:T(8,128)(2,1)S(1)} all-to-all(bf16[4,32,256]{2,1,0:T(8,128)(2,1)S(1)} %bitcast.215), channel_id=1, replica_groups=mesh['za'=4,'zb'=4,'zc'=2,'tp'=4,'dp'=8] {'tp'}, dimensions={0} | all-to-all | bytes 131072 | tf_op jit(solution)/shard_map/all_to_all | solution.py:316
  177.9 3.7 %fusion.1 = bf16[32,2048]{1,0:T(8,128)(2,1)} fusion(bf16[32,1024]{1,0:T(8,128)(2,1)S(1)} %bitcast.214, bf16[1024,2048]{1,0:T(8,128)(2,1)} %param.35, bf16[32,2048]{1,0:T(8,128)(2,1)S(1)} %copy-done.2, f32[2048]{0:T(1024)S(1)} %bitcast.230), kind=kOutput, calls=%fused_computation.2 | convolution fusion | flops 134479872 | bytes 4530176 | tf_op jit(solution)/shard_map/dot_general | solution.py:317
  (158 shorter events, 6.3 us)
Async XLA Ops:
  0.0 99.7 %copy-start = (bf16[2048,256]{1,0:T(8,128)(2,1)S(1)}, bf16[2048,256]{1,0:T(8,128)(2,1)}, u32[]{:S(2)}) copy-start(bf16[2048,256]{1,0:T(8,128)(2,1)} %param.24) | copy-start | bytes 3145732
  0.0 19.2 %copy-start.2 = (bf16[32,2048]{1,0:T(8,128)(2,1)S(1)}, bf16[32,2048]{1,0:T(8,128)(2,1)}, u32[]{:S(2)}) copy-start(bf16[32,2048]{1,0:T(8,128)(2,1)} %param.18) | copy-start | bytes 393220
  0.0 29.7 %copy-start.3 = (bf16[16,2048]{1,0:T(8,128)(2,1)S(1)}, bf16[16,2048]{1,0:T(8,128)(2,1)}, u32[]{:S(2)}) copy-start(bf16[16,2048]{1,0:T(8,128)(2,1)} %param.20) | copy-start | bytes 196612
  2.3 33.6 %all-to-all-start = ((f32[40,2,128]{2,1,0:T(2,128)}), f32[40,2,128]{2,1,0:T(2,128)S(1)}, u32[]{:S(2)}, u32[]{:S(2)}) async-start(f32[40,2,128]{2,1,0:T(2,128)} %partial_mods.1), calls=%async_computation | async-start | bytes 81920 | tf_op jit(solution)/shard_map/all_to_all | solution.py:27
  9.0 6.1 %collective-permute-start.1 = (bf16[16,2048]{1,0:T(8,128)(2,1)S(1)}, bf16[16,2048]{1,0:T(8,128)(2,1)S(1)}, u32[]{:S(2)}, u32[]{:S(2)}) collective-permute-start(bf16[16,2048]{1,0:T(8,128)(2,1)S(1)} %pad_maximum_fusion.13), channel_id=1, source_target_pairs={{0,32},{32,64},{64,96},{96,128},{128,160},{160,192},{192,224},{224... | collective-permute-start | bytes 196616 | tf_op jit(solution)/shard_map/ppermute | solution.py:231
  12.9 6.2 %collective-permute-start = (bf16[16,2048]{1,0:T(8,128)(2,1)S(1)}, bf16[16,2048]{1,0:T(8,128)(2,1)S(1)}, u32[]{:S(2)}, u32[]{:S(2)}) collective-permute-start(bf16[16,2048]{1,0:T(8,128)(2,1)S(1)} %pad_maximum_fusion.12), channel_id=1, source_target_pairs={{32,0},{64,32},{96,64},{128,96},{160,128},{192,160},{224,192},{256... | collective-permute-start | bytes 196616 | tf_op jit(solution)/shard_map/ppermute | solution.py:232
  19.2 11.3 %collective-permute-start.4 = (bf16[40,2048]{1,0:T(8,128)(2,1)S(1)}, bf16[40,2048]{1,0:T(8,128)(2,1)S(1)}, u32[]{:S(2)}, u32[]{:S(2)}) collective-permute-start(bf16[40,2048]{1,0:T(8,128)(2,1)S(1)} %get-tuple-element.42), channel_id=1, source_target_pairs={{0,24},{8,0},{16,8},{24,16},{1,25},{9,1},{17,9},{25,17},{2,26},{10... | collective-permute-start | bytes 491528 | tf_op jit(solution)/shard_map/ppermute | solution.py:38
  24.1 9.4 %collective-permute-start.3 = (bf16[40,2048]{1,0:T(8,128)(2,1)S(1)}, bf16[40,2048]{1,0:T(8,128)(2,1)S(1)}, u32[]{:S(2)}, u32[]{:S(2)}) collective-permute-start(bf16[40,2048]{1,0:T(8,128)(2,1)S(1)} %get-tuple-element.42), channel_id=1, source_target_pairs={{0,16},{8,24},{16,0},{24,8},{1,17},{9,25},{17,1},{25,9},{2,18},{10... | collective-permute-start | bytes 491528 | tf_op jit(solution)/shard_map/ppermute | solution.py:38
  26.9 8.5 %collective-permute-start.2 = (bf16[40,2048]{1,0:T(8,128)(2,1)S(1)}, bf16[40,2048]{1,0:T(8,128)(2,1)S(1)}, u32[]{:S(2)}, u32[]{:S(2)}) collective-permute-start(bf16[40,2048]{1,0:T(8,128)(2,1)S(1)} %get-tuple-element.42), channel_id=1, source_target_pairs={{0,8},{8,16},{16,24},{24,0},{1,9},{9,17},{17,25},{25,1},{2,10},{10... | collective-permute-start | bytes 491528 | tf_op jit(solution)/shard_map/ppermute | solution.py:38
  35.6 28.1 %copy-start.7 = (bf16[2,2048,4]{1,2,0:T(4,128)(2,1)S(1)}, bf16[2,2048,4]{1,2,0:T(4,128)(2,1)}, u32[]{:S(2)}) copy-start(bf16[2,2048,4]{1,2,0:T(4,128)(2,1)} %param.28) | copy-start | bytes 98308
  35.6 55.6 %copy-start.8 = (bf16[4,256]{1,0:T(4,128)(2,1)S(1)}, bf16[4,256]{1,0:T(4,128)(2,1)}, u32[]{:S(2)}) copy-start(bf16[4,256]{1,0:T(4,128)(2,1)} %param.29) | copy-start | bytes 6148
  35.6 55.6 %copy-start.9 = (bf16[2048]{0:T(1024)(128)(2,1)S(1)}, bf16[2048]{0:T(1024)(128)(2,1)}, u32[]{:S(2)}) copy-start(bf16[2048]{0:T(1024)(128)(2,1)} %param.23) | copy-start | bytes 12292
  35.6 55.6 %copy-start.13 = (f32[2,4]{1,0:T(2,128)S(1)}, f32[2,4]{1,0:T(2,128)}, u32[]{:S(2)}) copy-start(f32[2,4]{1,0:T(2,128)} %param.32) | copy-start | bytes 100
  35.6 55.7 %copy-start.18 = (bf16[256]{0:T(256)(128)(2,1)S(1)}, bf16[256]{0:T(256)(128)(2,1)}, u32[]{:S(2)}) copy-start(bf16[256]{0:T(256)(128)(2,1)} %param.34) | copy-start | bytes 1540
  35.7 55.7 %copy-start.10 = (bf16[4,64]{1,0:T(4,128)(2,1)S(1)}, bf16[4,64]{1,0:T(4,128)(2,1)}, u32[]{:S(2)}) copy-start(bf16[4,64]{1,0:T(4,128)(2,1)} %param.31) | copy-start | bytes 1540
  35.7 55.6 %copy-start.11 = (bf16[4,64]{1,0:T(4,128)(2,1)S(1)}, bf16[4,64]{1,0:T(4,128)(2,1)}, u32[]{:S(2)}) copy-start(bf16[4,64]{1,0:T(4,128)(2,1)} %param.30) | copy-start | bytes 1540
  36.6 50.5 %all-to-all-start.1 = ((f32[80,2,128]{2,1,0:T(2,128)}), f32[80,2,128]{2,1,0:T(2,128)S(1)}, u32[]{:S(2)}, u32[]{:S(2)}) async-start(f32[80,2,128]{2,1,0:T(2,128)} %bitcast.2), calls=%async_computation.1 | async-start | bytes 163840 | tf_op jit(solution)/shard_map/all_to_all | solution.py:27
  87.8 9.6 %all-to-all-start.2 = ((f32[40,2,128]{2,1,0:T(2,128)}), f32[40,2,128]{2,1,0:T(2,128)S(1)}, u32[]{:S(2)}, u32[]{:S(2)}) async-start(f32[40,2,128]{2,1,0:T(2,128)} %bitcast.4), calls=%async_computation.2 | async-start | bytes 81920 | tf_op jit(solution)/shard_map/all_to_all | solution.py:27
  97.5 1.0 copy-start.12
  97.5 1.5 copy-start.17
  102.3 5.5 %copy-start.4 = (bf16[2048,64]{0,1:T(8,128)(2,1)S(1)}, bf16[2048,64]{0,1:T(8,128)(2,1)}, u32[]{:S(2)}) copy-start(bf16[2048,64]{0,1:T(8,128)(2,1)} %param.27) | copy-start | bytes 786436
  104.2 15.1 %all-to-all-start.3 = ((bf16[8,72,128]{2,1,0:T(8,128)(2,1)}), bf16[8,72,128]{2,1,0:T(8,128)(2,1)S(1)}, u32[]{:S(2)}, u32[]{:S(2)}) async-start(bf16[8,72,128]{2,1,0:T(8,128)(2,1)} %pad_maximum_fusion.10), calls=%async_computation.3 | async-start | bytes 294912 | tf_op jit(solution)/shard_map/all_to_all | solution.py:27
  108.9 11.1 %copy-start.19 = (f32[128,128]{1,0:T(8,128)}, f32[128,128]{1,0:T(8,128)S(1)}, u32[]{:S(2)}) copy-start(f32[128,128]{1,0:T(8,128)S(1)} %fusion.144) | copy-start | bytes 196612
  110.6 18.7 %copy-start.14 = (f32[128]{0:T(128)S(1)}, f32[128]{0:T(128)}, u32[]{:S(2)}) copy-start(f32[128]{0:T(128)} %get-tuple-element.70) | copy-start | bytes 1540
  110.6 18.7 %copy-start.15 = (f32[128]{0:T(128)S(1)}, f32[128]{0:T(128)}, u32[]{:S(2)}) copy-start(f32[128]{0:T(128)} %get-tuple-element.71) | copy-start | bytes 1540
  110.6 18.7 %copy-start.16 = (f32[128]{0:T(128)S(1)}, f32[128]{0:T(128)}, u32[]{:S(2)}) copy-start(f32[128]{0:T(128)} %get-tuple-element.95) | copy-start | bytes 1540
  120.1 38.7 %copy-start.1 = (bf16[2048,256]{1,0:T(8,128)(2,1)S(1)}, bf16[2048,256]{1,0:T(8,128)(2,1)}, u32[]{:S(2)}) copy-start(bf16[2048,256]{1,0:T(8,128)(2,1)} %param.25) | copy-start | bytes 3145732
  120.7 31.6 %all-to-all-start.4 = ((bf16[4,72,128]{2,1,0:T(8,128)(2,1)}), bf16[4,72,128]{2,1,0:T(8,128)(2,1)S(1)}, u32[]{:S(2)}, u32[]{:S(2)}) async-start(bf16[4,72,128]{2,1,0:T(8,128)(2,1)} %broadcast_in_dim.615), calls=%async_computation.4 | async-start | bytes 147456 | tf_op jit(solution)/shard_map/all_to_all | solution.py:27
  153.6 14.4 %all-to-all-start.5 = ((bf16[8,32,128]{2,1,0:T(8,128)(2,1)}), bf16[8,32,128]{2,1,0:T(8,128)(2,1)S(1)}, u32[]{:S(2)}, u32[]{:S(2)}) async-start(bf16[8,32,128]{2,1,0:T(8,128)(2,1)} %fusion.28), calls=%async_computation.5 | async-start | bytes 131072 | tf_op jit(solution)/shard_map/all_to_all | solution.py:27
  158.8 9.6 %copy-start.5 = (f32[128,64]{1,0:T(8,128)S(1)}, f32[128,64]{1,0:T(8,128)}, u32[]{:S(2)}) copy-start(f32[128,64]{1,0:T(8,128)} %fusion.46) | copy-start | bytes 98308
  158.8 9.6 %copy-start.6 = (f32[128,64]{1,0:T(8,128)S(1)}, f32[128,64]{1,0:T(8,128)}, u32[]{:S(2)}) copy-start(f32[128,64]{1,0:T(8,128)} %fusion.48) | copy-start | bytes 98308
where the time goes:
time: 183 us; the launch traced here: 182 us
  waiting for transfers between devices  78.5 us (43%)
  starting transfers between devices  67.5 us (37%)
  matrix products  12.2 us (7%)
  blocking collectives  7.99 us (4%)
  local copies, waits for them, and re-layouts  7.22 us (4%)
  other arithmetic  4.98 us (3%)
  Pallas kernels  2.28 us (1%)
    all_to_all x6, waiting for transfers between devices, exchange(): return lax.all_to_all(x, axis, 0, 0, tiled=True)  68.9 us
    all_to_all x6, starting transfers between devices, exchange(): return lax.all_to_all(x, axis, 0, 0, tiled=True)  51.8 us
    ppermute x3, starting transfers between devices, ring_rows(): lax.ppermute(x, 'tp', [(i, (i + k) % n) for i in range(n)])  10.5 us
    all_to_all x1, blocking collectives, program(): lax.all_to_all(stacked, 'tp', split_axis=0, concat_axis=2, tiled=True)[0]  7.99 us
    ppermute x3, waiting for transfers between devices, ring_rows(): lax.ppermute(x, 'tp', [(i, (i + k) % n) for i in range(n)])  5.59 us
    dot_general x4, matrix products, program(): jnp.dot(weights, xs[:, h * HEAD_DIM:(h + 1) * HEAD_DIM], preferred_elemen...  4.48 us
    ppermute x1, waiting for transfers between devices, program(): lax.ppermute(jnp.concatenate([latent[:PAD], context[:PAD]]), SP, down)  4.04 us
    ppermute x1, starting transfers between devices, program(): low = lax.ppermute(jnp.concatenate([latent[-PAD:], context[-PAD:]]), SP, up)  3.93 us
  transfers between devices with their start and end apart: 11, of which 9 were waited for; matrix products, arithmetic and copies ran while one was open for 5% of the time, Pallas kernels for 0%

commit v1 on v0

--- a/solution.py
+++ b/solution.py
@@ -289,6 +289,7 @@
         total,
     )
 
+    cmat, w_early = lax.optimization_barrier((cmat, w_out[: w_out.shape[0] // 4]))
     affinity = lax.dot_general(cmat, bmat, (((1,), (1,)), ((), ())), preferred_element_type=F32)
     i = jnp.arange(tokens)
     lower = i[:, None] >= i[None, :]
@@ -314,7 +315,9 @@
     tp_count = lax.axis_size("tp")
     stacked = normed.reshape(tp_count, tokens // tp_count, head_cols)
     full = lax.all_to_all(stacked, "tp", split_axis=0, concat_axis=2, tiled=True)[0]
-    branch = jnp.dot(full, w_out, preferred_element_type=F32)
+    cut = w_early.shape[0]
+    branch = jnp.dot(full[:, :cut], w_early, preferred_element_type=F32)
+    branch = branch + jnp.dot(full[:, cut:], w_out[cut:], preferred_element_type=F32)
     return (latent.astype(F32) + mods[2] * branch).astype(BF16)
 
 

time: 183 us -> 183 us (level)
  starting transfers between devices: 67.5 us -> 75.5 us
  waiting for transfers between devices: 78.5 us -> 71.6 us
    all_to_all x6, starting transfers between devices: 51.8 us -> 57.2 us  [exchange(): return lax.all_to_all(x, axis, 0, 0, tiled=True)]
    ppermute x1, waiting for transfers between devices: 4.04 us -> 0.01 us  [program(): lax.ppermute(jnp.concatenate([latent[:PAD], context[:PAD]]), SP, down)]
    ppermute x3, waiting for transfers between devices: 5.59 us -> 2.65 us  [ring_rows(): lax.ppermute(x, 'tp', [(i, (i + k) % n) for i in range(n)])]
    ppermute x3, starting transfers between devices: 10.5 us -> 12.5 us  [ring_rows(): lax.ppermute(x, 'tp', [(i, (i + k) % n) for i in range(n)])]
    dot_general x1 -> x2, matrix products: 3.68 us -> 3.57 us  [the longest x1 2.61 us: program(): jnp.dot(full[:, cut:], w_out[cut:], preferred_element_type=F32)]
  transfers between devices with their start and end apart: 11 -> 11, of which waited for: 9 -> 8; matrix products, arithmetic and copies ran while one was open for 5% -> 5% of each run, Pallas kernels for 0% -> 0%
where the time goes in v1:
time: 183 us; the launch traced here: 182 us
  starting transfers between devices  75.5 us (41%)
  waiting for transfers between devices  71.6 us (39%)
  matrix products  12.8 us (7%)
  blocking collectives  7.99 us (4%)
  local copies, waits for them, and re-layouts  5.56 us (3%)
  other arithmetic  4.99 us (3%)
  Pallas kernels  2.27 us (1%)
    all_to_all x6, waiting for transfers between devices, exchange(): return lax.all_to_all(x, axis, 0, 0, tiled=True)  67.9 us
    all_to_all x6, starting transfers between devices, exchange(): return lax.all_to_all(x, axis, 0, 0, tiled=True)  57.2 us
    ppermute x3, starting transfers between devices, ring_rows(): lax.ppermute(x, 'tp', [(i, (i + k) % n) for i in range(n)])  12.5 us
    all_to_all x1, blocking collectives, program(): lax.all_to_all(stacked, 'tp', split_axis=0, concat_axis=2, tiled=True)[0]  7.99 us
    dot_general x4, matrix products, program(): jnp.dot(weights, xs[:, h * HEAD_DIM:(h + 1) * HEAD_DIM], preferred_elemen...  5.13 us
    ppermute x1, starting transfers between devices, program(): low = lax.ppermute(jnp.concatenate([latent[-PAD:], context[-PAD:]]), SP, up)  4.56 us
  transfers between devices with their start and end apart: 11, of which 8 were waited for; matrix products, arithmetic and copies ran while one was open for 5% of the time, Pallas kernels for 0%

profile of v1, /device:TPU:2, one launch (start us, length us, event | category | flops | bytes accessed | tf_op | source)
XLA Modules:
  0.0 181.6 jit_solution(870321081223710214)
XLA Ops:
  0.0 2.3 %partial_mods.1 = f32[40,2,128]{2,1,0:T(2,128)} custom-call(s32[1]{0:T(128)} %bitcast.first, bf16[2048]{0:T(1024)(128)(2,1)} %cond.1, bf16[2048]{0:T(1024)(128)(2,1)} %context_cond.1, bf16[16,6144]{1,0:T(8,128)(2,1)} %modulation.1), custom_call_target="tpu_custom_call" | custom-call | tf_op jit(solution)/shard_map/partial_mods/pallas_call | solution.py:77
  2.3 5.8 %all-to-all-start = ((f32[40,2,128]{2,1,0:T(2,128)}), f32[40,2,128]{2,1,0:T(2,128)S(1)}, u32[]{:S(2)}, u32[]{:S(2)}) async-start(f32[40,2,128]{2,1,0:T(2,128)} %partial_mods.1), calls=%async_computation | async-start | bytes 81920 | tf_op jit(solution)/shard_map/all_to_all | solution.py:27
  8.1 0.8 fusion.141
  8.9 1.3 collective-permute-start
  10.2 4.6 %collective-permute-start.1 = (bf16[16,2048]{1,0:T(8,128)(2,1)S(1)}, bf16[16,2048]{1,0:T(8,128)(2,1)S(1)}, u32[]{:S(2)}, u32[]{:S(2)}) collective-permute-start(bf16[16,2048]{1,0:T(8,128)(2,1)S(1)} %pad_maximum_fusion.13), channel_id=1, source_target_pairs={{0,32},{32,64},{64,96},{96,128},{128,160},{160,192},{192,224},{224... | collective-permute-start | bytes 196616 | tf_op jit(solution)/shard_map/ppermute | solution.py:231
  15.7 1.0 collective-permute-done.1
  16.8 5.4 %collective-permute-start.3 = (bf16[40,2048]{1,0:T(8,128)(2,1)S(1)}, bf16[40,2048]{1,0:T(8,128)(2,1)S(1)}, u32[]{:S(2)}, u32[]{:S(2)}) collective-permute-start(bf16[40,2048]{1,0:T(8,128)(2,1)S(1)} %get-tuple-element.46), channel_id=1, source_target_pairs={{0,16},{8,24},{16,0},{24,8},{1,17},{9,25},{17,1},{25,9},{2,18},{10... | collective-permute-start | bytes 491528 | tf_op jit(solution)/shard_map/ppermute | solution.py:38
  22.2 2.5 %collective-permute-start.2 = (bf16[40,2048]{1,0:T(8,128)(2,1)S(1)}, bf16[40,2048]{1,0:T(8,128)(2,1)S(1)}, u32[]{:S(2)}, u32[]{:S(2)}) collective-permute-start(bf16[40,2048]{1,0:T(8,128)(2,1)S(1)} %get-tuple-element.46), channel_id=1, source_target_pairs={{0,8},{8,16},{16,24},{24,0},{1,9},{9,17},{17,25},{25,1},{2,10},{10... | collective-permute-start | bytes 491528 | tf_op jit(solution)/shard_map/ppermute | solution.py:38
  24.7 4.6 %collective-permute-start.4 = (bf16[40,2048]{1,0:T(8,128)(2,1)S(1)}, bf16[40,2048]{1,0:T(8,128)(2,1)S(1)}, u32[]{:S(2)}, u32[]{:S(2)}) collective-permute-start(bf16[40,2048]{1,0:T(8,128)(2,1)S(1)} %get-tuple-element.46), channel_id=1, source_target_pairs={{0,24},{8,0},{16,8},{24,16},{1,25},{9,1},{17,9},{25,17},{2,26},{10... | collective-permute-start | bytes 491528 | tf_op jit(solution)/shard_map/ppermute | solution.py:38
  29.5 1.2 collective-permute-done.2
  30.7 1.5 collective-permute-done.4
  32.4 0.2 fusion.5
  32.7 0.7 broadcast_in_dim.554
  33.3 29.6 %all-to-all-start.1 = ((f32[80,2,128]{2,1,0:T(2,128)}), f32[80,2,128]{2,1,0:T(2,128)S(1)}, u32[]{:S(2)}, u32[]{:S(2)}) async-start(f32[80,2,128]{2,1,0:T(2,128)} %bitcast.2), calls=%async_computation.1 | async-start | bytes 163840 | tf_op jit(solution)/shard_map/all_to_all | solution.py:27
  63.0 22.7 %all-to-all-done.1 = f32[80,2,128]{2,1,0:T(2,128)S(1)} async-done(((f32[80,2,128]{2,1,0:T(2,128)}), f32[80,2,128]{2,1,0:T(2,128)S(1)}, u32[]{:S(2)}, u32[]{:S(2)}) %all-to-all-start.1) | async-done | bytes 81952 | tf_op jit(solution)/shard_map/all_to_all | solution.py:27
  85.8 0.6 broadcast_in_dim.555
  86.4 4.9 %all-to-all-start.2 = ((f32[40,2,128]{2,1,0:T(2,128)}), f32[40,2,128]{2,1,0:T(2,128)S(1)}, u32[]{:S(2)}, u32[]{:S(2)}) async-start(f32[40,2,128]{2,1,0:T(2,128)} %bitcast.4), calls=%async_computation.2 | async-start | bytes 81920 | tf_op jit(solution)/shard_map/all_to_all | solution.py:27
  91.4 6.1 %all-to-all-done.2 = f32[40,2,128]{2,1,0:T(2,128)S(1)} async-done(((f32[40,2,128]{2,1,0:T(2,128)}), f32[40,2,128]{2,1,0:T(2,128)S(1)}, u32[]{:S(2)}, u32[]{:S(2)}) %all-to-all-start.2) | async-done | bytes 40992 | tf_op jit(solution)/shard_map/all_to_all | solution.py:27
  97.8 0.3 fusion.9
  98.1 0.3 compare_select_fusion
  98.4 0.2 fusion.139
  98.8 0.2 fusion.138
  99.3 0.4 fusion.17
  99.8 0.4 fusion.11
  101.8 0.2 fusion.19
  102.4 0.2 fusion.18
  102.7 0.7 pad_maximum_fusion.10
  103.4 3.7 %all-to-all-start.3 = ((bf16[8,72,128]{2,1,0:T(8,128)(2,1)}), bf16[8,72,128]{2,1,0:T(8,128)(2,1)S(1)}, u32[]{:S(2)}, u32[]{:S(2)}) async-start(bf16[8,72,128]{2,1,0:T(8,128)(2,1)} %pad_maximum_fusion.10), calls=%async_computation.3 | async-start | bytes 294912 | tf_op jit(solution)/shard_map/all_to_all | solution.py:27
  107.1 0.3 fusion.21
  107.6 0.2 fusion.149
  107.7 0.9 fusion.50
  108.6 0.9 fusion.52
  109.5 9.3 %all-to-all-done.3 = bf16[8,72,128]{2,1,0:T(8,128)(2,1)S(1)} async-done(((bf16[8,72,128]{2,1,0:T(8,128)(2,1)}), bf16[8,72,128]{2,1,0:T(8,128)(2,1)S(1)}, u32[]{:S(2)}, u32[]{:S(2)}) %all-to-all-start.3) | async-done | bytes 147488 | tf_op jit(solution)/shard_map/all_to_all | solution.py:27
  118.8 0.3 fusion.24
  119.5 0.6 broadcast_in_dim.615
  120.2 8.7 %all-to-all-start.4 = ((bf16[4,72,128]{2,1,0:T(8,128)(2,1)}), bf16[4,72,128]{2,1,0:T(8,128)(2,1)S(1)}, u32[]{:S(2)}, u32[]{:S(2)}) async-start(bf16[4,72,128]{2,1,0:T(8,128)(2,1)} %broadcast_in_dim.615), calls=%async_computation.4 | async-start | bytes 147456 | tf_op jit(solution)/shard_map/all_to_all | solution.py:27
  128.9 1.7 fusion.54
  130.6 21.0 %all-to-all-done.4 = bf16[4,72,128]{2,1,0:T(8,128)(2,1)S(1)} async-done(((bf16[4,72,128]{2,1,0:T(8,128)(2,1)}), bf16[4,72,128]{2,1,0:T(8,128)(2,1)S(1)}, u32[]{:S(2)}, u32[]{:S(2)}) %all-to-all-start.4) | async-done | bytes 73760 | tf_op jit(solution)/shard_map/all_to_all | solution.py:27
  152.1 0.6 fusion.31
  152.8 4.4 %all-to-all-start.5 = ((bf16[8,32,128]{2,1,0:T(8,128)(2,1)}), bf16[8,32,128]{2,1,0:T(8,128)(2,1)S(1)}, u32[]{:S(2)}, u32[]{:S(2)}) async-start(bf16[8,32,128]{2,1,0:T(8,128)(2,1)} %fusion.31), calls=%async_computation.5 | async-start | bytes 131072 | tf_op jit(solution)/shard_map/all_to_all | solution.py:27
  157.2 1.7 fusion.56
  158.9 0.3 fusion.15
  159.2 8.9 %all-to-all-done.5 = bf16[8,32,128]{2,1,0:T(8,128)(2,1)S(1)} async-done(((bf16[8,32,128]{2,1,0:T(8,128)(2,1)}), bf16[8,32,128]{2,1,0:T(8,128)(2,1)S(1)}, u32[]{:S(2)}, u32[]{:S(2)}) %all-to-all-start.5) | async-done | bytes 65568 | tf_op jit(solution)/shard_map/all_to_all | solution.py:27
  168.5 1.1 fusion.14
  169.6 0.2 multiply_reduce_fusion.4
  170.0 8.0 %all_to_all.46 = bf16[4,32,256]{2,1,0:T(8,128)(2,1)S(1)} all-to-all(bf16[4,32,256]{2,1,0:T(8,128)(2,1)S(1)} %bitcast.215), channel_id=1, replica_groups=mesh['za'=4,'zb'=4,'zc'=2,'tp'=4,'dp'=8] {'tp'}, dimensions={0} | all-to-all | bytes 131072 | tf_op jit(solution)/shard_map/all_to_all | solution.py:317
  178.0 2.6 %fusion = f32[32,2048]{1,0:T(8,128)S(1)} fusion(bf16[1024,2048]{1,0:T(8,128)(2,1)} %param.35, bf16[32,1024]{1,0:T(8,128)(2,1)S(1)} %bitcast.213), kind=kOutput, calls=%fused_computation | convolution fusion | flops 100663296 | bytes 3457024 | tf_op jit(solution)/shard_map/dot_general | solution.py:320
  180.7 1.0 fusion.4
  (151 shorter events, 5.9 us)
Async XLA Ops:
  0.0 99.8 %copy-start = (bf16[2048,256]{1,0:T(8,128)(2,1)S(1)}, bf16[2048,256]{1,0:T(8,128)(2,1)}, u32[]{:S(2)}) copy-start(bf16[2048,256]{1,0:T(8,128)(2,1)} %param.24) | copy-start | bytes 3145732
  2.3 30.4 %all-to-all-start = ((f32[40,2,128]{2,1,0:T(2,128)}), f32[40,2,128]{2,1,0:T(2,128)S(1)}, u32[]{:S(2)}, u32[]{:S(2)}) async-start(f32[40,2,128]{2,1,0:T(2,128)} %partial_mods.1), calls=%async_computation | async-start | bytes 81920 | tf_op jit(solution)/shard_map/all_to_all | solution.py:27
  8.9 6.7 %collective-permute-start = (bf16[16,2048]{1,0:T(8,128)(2,1)S(1)}, bf16[16,2048]{1,0:T(8,128)(2,1)S(1)}, u32[]{:S(2)}, u32[]{:S(2)}) collective-permute-start(bf16[16,2048]{1,0:T(8,128)(2,1)S(1)} %pad_maximum_fusion.12), channel_id=1, source_target_pairs={{32,0},{64,32},{96,64},{128,96},{160,128},{192,160},{224,192},{256... | collective-permute-start | bytes 196616 | tf_op jit(solution)/shard_map/ppermute | solution.py:232
  10.2 6.5 %collective-permute-start.1 = (bf16[16,2048]{1,0:T(8,128)(2,1)S(1)}, bf16[16,2048]{1,0:T(8,128)(2,1)S(1)}, u32[]{:S(2)}, u32[]{:S(2)}) collective-permute-start(bf16[16,2048]{1,0:T(8,128)(2,1)S(1)} %pad_maximum_fusion.13), channel_id=1, source_target_pairs={{0,32},{32,64},{64,96},{96,128},{128,160},{160,192},{192,224},{224... | collective-permute-start | bytes 196616 | tf_op jit(solution)/shard_map/ppermute | solution.py:231
  15.2 1.6 copy-start.2
  15.6 13.7 %copy-start.3 = (bf16[16,2048]{1,0:T(8,128)(2,1)S(1)}, bf16[16,2048]{1,0:T(8,128)(2,1)}, u32[]{:S(2)}) copy-start(bf16[16,2048]{1,0:T(8,128)(2,1)} %param.20) | copy-start | bytes 196612
  16.8 12.7 %collective-permute-start.3 = (bf16[40,2048]{1,0:T(8,128)(2,1)S(1)}, bf16[40,2048]{1,0:T(8,128)(2,1)S(1)}, u32[]{:S(2)}, u32[]{:S(2)}) collective-permute-start(bf16[40,2048]{1,0:T(8,128)(2,1)S(1)} %get-tuple-element.46), channel_id=1, source_target_pairs={{0,16},{8,24},{16,0},{24,8},{1,17},{9,25},{17,1},{25,9},{2,18},{10... | collective-permute-start | bytes 491528 | tf_op jit(solution)/shard_map/ppermute | solution.py:38
  22.2 8.4 %collective-permute-start.2 = (bf16[40,2048]{1,0:T(8,128)(2,1)S(1)}, bf16[40,2048]{1,0:T(8,128)(2,1)S(1)}, u32[]{:S(2)}, u32[]{:S(2)}) collective-permute-start(bf16[40,2048]{1,0:T(8,128)(2,1)S(1)} %get-tuple-element.46), channel_id=1, source_target_pairs={{0,8},{8,16},{16,24},{24,0},{1,9},{9,17},{17,25},{25,1},{2,10},{10... | collective-permute-start | bytes 491528 | tf_op jit(solution)/shard_map/ppermute | solution.py:38
  24.7 7.4 %collective-permute-start.4 = (bf16[40,2048]{1,0:T(8,128)(2,1)S(1)}, bf16[40,2048]{1,0:T(8,128)(2,1)S(1)}, u32[]{:S(2)}, u32[]{:S(2)}) collective-permute-start(bf16[40,2048]{1,0:T(8,128)(2,1)S(1)} %get-tuple-element.46), channel_id=1, source_target_pairs={{0,24},{8,0},{16,8},{24,16},{1,25},{9,1},{17,9},{25,17},{2,26},{10... | collective-permute-start | bytes 491528 | tf_op jit(solution)/shard_map/ppermute | solution.py:38
  32.3 30.7 %copy-start.5 = (bf16[2,2048,4]{1,2,0:T(4,128)(2,1)S(1)}, bf16[2,2048,4]{1,2,0:T(4,128)(2,1)}, u32[]{:S(2)}) copy-start(bf16[2,2048,4]{1,2,0:T(4,128)(2,1)} %param.28) | copy-start | bytes 98308
  32.3 59.0 %copy-start.6 = (bf16[4,256]{1,0:T(4,128)(2,1)S(1)}, bf16[4,256]{1,0:T(4,128)(2,1)}, u32[]{:S(2)}) copy-start(bf16[4,256]{1,0:T(4,128)(2,1)} %param.29) | copy-start | bytes 6148
  32.3 59.0 %copy-start.11 = (f32[2,4]{1,0:T(2,128)S(1)}, f32[2,4]{1,0:T(2,128)}, u32[]{:S(2)}) copy-start(f32[2,4]{1,0:T(2,128)} %param.32) | copy-start | bytes 100
  32.3 59.1 %copy-start.13 = (bf16[256]{0:T(256)(128)(2,1)S(1)}, bf16[256]{0:T(256)(128)(2,1)}, u32[]{:S(2)}) copy-start(bf16[256]{0:T(256)(128)(2,1)} %param.34) | copy-start | bytes 1540
  32.3 59.0 %copy-start.7 = (bf16[2048]{0:T(1024)(128)(2,1)S(1)}, bf16[2048]{0:T(1024)(128)(2,1)}, u32[]{:S(2)}) copy-start(bf16[2048]{0:T(1024)(128)(2,1)} %param.23) | copy-start | bytes 12292
  32.4 59.0 %copy-start.8 = (bf16[4,64]{1,0:T(4,128)(2,1)S(1)}, bf16[4,64]{1,0:T(4,128)(2,1)}, u32[]{:S(2)}) copy-start(bf16[4,64]{1,0:T(4,128)(2,1)} %param.31) | copy-start | bytes 1540
  32.4 59.0 %copy-start.9 = (bf16[4,64]{1,0:T(4,128)(2,1)S(1)}, bf16[4,64]{1,0:T(4,128)(2,1)}, u32[]{:S(2)}) copy-start(bf16[4,64]{1,0:T(4,128)(2,1)} %param.30) | copy-start | bytes 1540
  33.3 52.4 %all-to-all-start.1 = ((f32[80,2,128]{2,1,0:T(2,128)}), f32[80,2,128]{2,1,0:T(2,128)S(1)}, u32[]{:S(2)}, u32[]{:S(2)}) async-start(f32[80,2,128]{2,1,0:T(2,128)} %bitcast.2), calls=%async_computation.1 | async-start | bytes 163840 | tf_op jit(solution)/shard_map/all_to_all | solution.py:27
  86.4 11.2 %all-to-all-start.2 = ((f32[40,2,128]{2,1,0:T(2,128)}), f32[40,2,128]{2,1,0:T(2,128)S(1)}, u32[]{:S(2)}, u32[]{:S(2)}) async-start(f32[40,2,128]{2,1,0:T(2,128)} %bitcast.4), calls=%async_computation.2 | async-start | bytes 81920 | tf_op jit(solution)/shard_map/all_to_all | solution.py:27
  97.7 1.1 copy-start.10
  97.8 1.6 copy-start.12
  102.0 5.1 %copy-start.4 = (bf16[2048,64]{0,1:T(8,128)(2,1)S(1)}, bf16[2048,64]{0,1:T(8,128)(2,1)}, u32[]{:S(2)}) copy-start(bf16[2048,64]{0,1:T(8,128)(2,1)} %param.27) | copy-start | bytes 786436
  103.4 15.4 %all-to-all-start.3 = ((bf16[8,72,128]{2,1,0:T(8,128)(2,1)}), bf16[8,72,128]{2,1,0:T(8,128)(2,1)S(1)}, u32[]{:S(2)}, u32[]{:S(2)}) async-start(bf16[8,72,128]{2,1,0:T(8,128)(2,1)} %pad_maximum_fusion.10), calls=%async_computation.3 | async-start | bytes 294912 | tf_op jit(solution)/shard_map/all_to_all | solution.py:27
  107.7 11.3 %copy-start.14 = (f32[128,128]{1,0:T(8,128)}, f32[128,128]{1,0:T(8,128)S(1)}, u32[]{:S(2)}) copy-start(f32[128,128]{1,0:T(8,128)S(1)} %fusion.149) | copy-start | bytes 196612
  119.5 39.4 %copy-start.1 = (bf16[2048,256]{1,0:T(8,128)(2,1)S(1)}, bf16[2048,256]{1,0:T(8,128)(2,1)}, u32[]{:S(2)}) copy-start(bf16[2048,256]{1,0:T(8,128)(2,1)} %param.25) | copy-start | bytes 3145732
  120.2 31.4 %all-to-all-start.4 = ((bf16[4,72,128]{2,1,0:T(8,128)(2,1)}), bf16[4,72,128]{2,1,0:T(8,128)(2,1)S(1)}, u32[]{:S(2)}, u32[]{:S(2)}) async-start(bf16[4,72,128]{2,1,0:T(8,128)(2,1)} %broadcast_in_dim.615), calls=%async_computation.4 | async-start | bytes 147456 | tf_op jit(solution)/shard_map/all_to_all | solution.py:27
  152.8 15.3 %all-to-all-start.5 = ((bf16[8,32,128]{2,1,0:T(8,128)(2,1)}), bf16[8,32,128]{2,1,0:T(8,128)(2,1)S(1)}, u32[]{:S(2)}, u32[]{:S(2)}) async-start(bf16[8,32,128]{2,1,0:T(8,128)(2,1)} %fusion.31), calls=%async_computation.5 | async-start | bytes 131072 | tf_op jit(solution)/shard_map/all_to_all | solution.py:27
  178.0 2.6 %slice-start = ((bf16[1024,2048]{1,0:T(8,128)(2,1)}), bf16[256,2048]{1,0:T(8,128)(2,1)S(1)}, s32[]{:S(2)}) async-start(bf16[1024,2048]{1,0:T(8,128)(2,1)} %param.35), calls=%async_computation.7 | async-start | bytes 2097152 | tf_op jit(solution)/shard_map/slice | solution.py:292
